TPU v7x, 512 devices: a 8x2x16 block of a 8x8x16 slice. The times are simulated.
512 devices in a mesh: grp: 2 (over y), dp: 8 (over x), kv: 16 (over z), tp: 2 (over core).
Axes of the slice: x: 8, y: 2, z: 16, core: 2. Of those that a mesh axis runs over, the one named last changes fastest.
The devices are a block of a 8x8x16 slice.
Arguments:
- tokens: bfloat16 [384, 4, 4096], P(('grp', 'dp'), None, ('kv', 'tp')), parts along dimension 0, may hold values from -6 to 6
- norm_gain: float32 [4096], replicated, may hold values from 0.1 to 1.9
- w_query: bfloat16 [16, 128, 4096], P('kv', 'tp'), may hold values from -0.09375 to 0.09375
- w_key: bfloat16 [16, 128, 4096], P('kv', 'tp'), may hold values from -0.09375 to 0.09375
- w_value: bfloat16 [16, 128, 4096], P('kv', 'tp'), may hold values from -0.09375 to 0.09375
- w_gate: bfloat16 [16, 128, 4096], P('kv', 'tp'), may hold values from -0.09375 to 0.09375
- w_decay: bfloat16 [4096, 16], replicated, may hold values from -0.09375 to 0.09375
- w_beta: bfloat16 [4096, 16], replicated, may hold values from -0.09375 to 0.09375
- decay_rate: float32 [16], P('kv'), may hold values from 0.02 to 1
- head_gain: float32 [128], P('tp'), may hold values from 0.1 to 1.9
- w_out: bfloat16 [16, 128, 4096], P('kv', 'tp'), may hold values from -0.1875 to 0.1875
- state: float32 [384, 16, 128, 128], P(('grp', 'dp'), 'kv', 'tp'), parts along dimension 0, may hold values from -6 to 6
- prev_keys: bfloat16 [384, 4, 16, 128], P(('grp', 'dp'), None, 'kv'), parts along dimension 0, may hold values from -6 to 6
- prev_values: bfloat16 [384, 4, 16, 128], P(('grp', 'dp'), None, 'kv', 'tp'), parts along dimension 0, may hold values from -6 to 6
- prev_decay: float32 [384, 4, 16], P(('grp', 'dp'), None, 'kv'), parts along dimension 0, may hold values from 0.01 to 1
- prev_beta: float32 [384, 4, 16], P(('grp', 'dp'), None, 'kv'), parts along dimension 0, may hold values from 0.05 to 1
- accepted: int32 [384], P(('grp', 'dp')), parts along dimension 0, may hold values from 0 to 4
Outputs:
- mixed: bfloat16 [384, 4, 4096], P(('grp', 'dp'), None, ('kv', 'tp')), parts along dimension 0
- committed: float32 [384, 16, 128, 128], P(('grp', 'dp'), 'kv', 'tp'), parts along dimension 0
There are 2 independent parts, one for each index of `grp`. A program takes and returns all parts, laid end to end along the dimension named above; an argument that names none is the same for every part. Nothing has to cross between parts.
All inputs are finite; a program needn't handle non-finite values.
Results may differ from a plain program's by a relative error of at most 0.015.
Values may be sent and summed in bfloat16 or wider, within the bound.
No kernel may reach another device: no remote copies, remote signals or barrier semaphores. Data moves between devices by JAX's collectives and lax.ppermute only.
A program may use at most 64 MiB of HBM per device.

v0:
```python
import jax
import jax.numpy as jnp
from jax import lax
from jax.sharding import PartitionSpec as P

DK = 128
DV = 128
EPS = 1e-06
PRECISE = lax.Precision.HIGHEST


def joined_along(parts, dim):
    parts = jnp.moveaxis(parts, 0, dim)
    shape = parts.shape
    return parts.reshape(*shape[:dim], shape[dim] * shape[dim + 1], *shape[dim + 2 :])


def gather_in_order(array, axes, sequence):
    parts = array[None]
    for k in sequence:
        parts = lax.all_gather(parts, axes[k], axis=0, tiled=True)
    current = [lax.axis_size(axes[k]) for k in reversed(sequence)]
    parts = parts.reshape(*current, *array.shape)
    turned = sorted(range(len(sequence)), key=lambda place: sequence[len(sequence) - 1 - place])
    return parts.transpose(*turned, *range(len(sequence), parts.ndim)).reshape(-1, *array.shape)


def gather_axes(array, axes, sequence, dim):
    return joined_along(gather_in_order(array, axes, sequence), dim)


def rows_first(arrays, axis, dims):
    turned = [jnp.moveaxis(a, dim, 0) for a, dim in zip(arrays, dims)]
    both = jnp.concatenate([t.reshape(len(t), -1) for t in turned], axis=1)
    out, at, finished = (lax.all_gather(both, axis, axis=0, tiled=True), 0, [])
    for t, dim in zip(turned, dims):
        share = out[:, at : at + t[0].size].reshape(-1, *t.shape[1:])
        finished.append(jnp.moveaxis(share, 0, dim))
        at += t[0].size
    return tuple(finished)


def total_of_pieces(array, axis):
    parts = lax.all_gather(array, axis)
    return parts.sum(axis=0)


def from_everyone(array, axis):
    copies = jnp.broadcast_to(array, (lax.axis_size(axis), *array.shape))
    return lax.all_to_all(copies, axis, split_axis=0, concat_axis=0, tiled=True)


def gathered_copies(array, axis, dim):
    parts = from_everyone(array, axis)
    return joined_along(parts, dim)


def from_partner(block, axis, bit):
    count = lax.axis_size(axis)
    route = []
    for low in range(count):
        high = low | 1 << bit
        if high != low and high < count:
            route += [(low, high), (high, low)]
    return lax.ppermute(block, axis, route)


def split_up(array, dim, devices):
    shape = array.shape
    parts = array.reshape(*shape[:dim], devices, shape[dim] // devices, *shape[dim + 1 :])
    return jnp.moveaxis(parts, dim, 0)


def sum_at_owner(array, axis, dim):
    parts = split_up(array, dim, lax.axis_size(axis))
    arrived = lax.all_to_all(parts, axis, split_axis=0, concat_axis=0, tiled=True)
    return arrived.astype(jnp.float32).sum(axis=0)


def unit_rows(values):
    return values * lax.rsqrt(jnp.sum(values * values, axis=-1, keepdims=True) + EPS)


def delta_update(carried, keys_now, values_now, retain, strength):
    carried = carried * retain[..., None, None]
    predicted = jnp.einsum("shed,shd->she", carried, keys_now, precision=PRECISE)
    update = strength[..., None] * (values_now - predicted)
    return carried + update[..., :, None] * keys_now[..., None, :]


def local(
    tokens,
    norm_gain,
    w_query,
    w_key,
    w_value,
    w_gate,
    w_decay,
    w_beta,
    decay_rate,
    head_gain,
    w_out,
    state,
    prev_keys,
    prev_values,
    prev_decay,
    prev_beta,
    accepted,
):
    gathered = gather_axes(tokens, ("kv", "tp"), (0, 1), 2)
    seq_local, proposals, width = gathered.shape
    row_count = seq_local * proposals
    floats = gathered.astype(jnp.float32)
    normed = (
        floats * lax.rsqrt(jnp.mean(floats * floats, axis=-1, keepdims=True) + EPS) * norm_gain
    ).astype(jnp.bfloat16)
    flat_rows = normed.reshape(row_count, width)
    heads_local = w_query.shape[0]

    def project(weight):
        product = lax.dot_general(
            flat_rows,
            weight.reshape(-1, width),
            (((1,), (1,)), ((), ())),
            preferred_element_type=jnp.float32,
        )
        return product.astype(jnp.bfloat16).reshape(seq_local, proposals, heads_local, -1)

    query_half = project(w_query)
    key_half = project(w_key)
    value_raw = project(w_value)
    gate_raw = project(w_gate)
    query_full, key_full = rows_first((query_half, key_half), "tp", (3, 3))
    head_start = lax.axis_index("kv") * heads_local
    decay_all = jnp.dot(flat_rows, w_decay, preferred_element_type=jnp.float32)
    beta_all = jnp.dot(flat_rows, w_beta, preferred_element_type=jnp.float32)
    decay_pre = lax.dynamic_slice_in_dim(decay_all, head_start, heads_local, 1).reshape(
        seq_local, proposals, heads_local
    )
    beta_pre = lax.dynamic_slice_in_dim(beta_all, head_start, heads_local, 1).reshape(
        seq_local, proposals, heads_local
    )
    forget = decay_rate * jax.nn.softplus(decay_pre)
    strength = jax.nn.sigmoid(beta_pre)
    queries = unit_rows(jax.nn.silu(query_full.astype(jnp.float32))) * DK ** (-0.5)
    key_unit = unit_rows(jax.nn.silu(key_full.astype(jnp.float32)))
    value_act = jax.nn.silu(value_raw.astype(jnp.float32))
    old_keys = unit_rows(prev_keys.astype(jnp.float32))
    old_values = prev_values.astype(jnp.float32)
    carried = state
    for position in range(proposals):
        accept_mask = (position < accepted).astype(jnp.float32)[:, None]
        carried = delta_update(
            carried,
            old_keys[:, position],
            old_values[:, position],
            jnp.exp(-prev_decay[:, position] * accept_mask),
            prev_beta[:, position] * accept_mask,
        )
    committed = carried
    outputs = []
    for position in range(proposals):
        carried = delta_update(
            carried,
            key_unit[:, position],
            value_act[:, position],
            jnp.exp(-forget[:, position]),
            strength[:, position],
        )
        outputs.append(
            jnp.einsum("shed,shd->she", carried, queries[:, position], precision=PRECISE)
        )
    heads_out = jnp.stack(outputs, axis=1)
    squares = total_of_pieces(jnp.sum(heads_out * heads_out, axis=-1), "tp")
    scaled = (
        heads_out
        * lax.rsqrt(squares[..., None] / DV + EPS)
        * head_gain
        * jax.nn.silu(gate_raw.astype(jnp.float32))
    ).astype(jnp.bfloat16)
    head_values = gathered_copies(scaled, "tp", 3)
    own_half = lax.axis_index("tp")
    kv_count = lax.axis_size("kv")
    col_block = w_out.shape[-1] // (kv_count * 2)
    grouped = w_out.reshape(heads_local, w_out.shape[1], kv_count, 2, col_block)
    own_rows = lax.dynamic_index_in_dim(grouped, own_half, 3, keepdims=False)
    other_rows = lax.dynamic_index_in_dim(grouped, 1 - own_half, 3, keepdims=False)
    received = from_partner(other_rows, "tp", 0)
    stacked = jnp.where(
        own_half == 0,
        jnp.concatenate([own_rows, received], axis=1),
        jnp.concatenate([received, own_rows], axis=1),
    )
    partial_value = jnp.dot(
        head_values.reshape(row_count, -1),
        stacked.reshape(-1, kv_count * col_block),
        preferred_element_type=jnp.float32,
    )
    mixed_out = sum_at_owner(partial_value.astype(jnp.bfloat16), "kv", 1)
    return (mixed_out.astype(jnp.bfloat16).reshape(seq_local, proposals, -1), committed)


def solution(mesh):
    in_specs = (
        P(("grp", "dp"), None, ("kv", "tp")),
        P(),
        P("kv", "tp", None),
        P("kv", "tp", None),
        P("kv", "tp", None),
        P("kv", "tp", None),
        P(),
        P(),
        P("kv"),
        P("tp"),
        P("kv", "tp", None),
        P(("grp", "dp"), "kv", "tp", None),
        P(("grp", "dp"), None, "kv", None),
        P(("grp", "dp"), None, "kv", "tp"),
        P(("grp", "dp"), None, "kv"),
        P(("grp", "dp"), None, "kv"),
        P(("grp", "dp")),
    )
    out_specs = (P(("grp", "dp"), None, ("kv", "tp")), P(("grp", "dp"), "kv", "tp", None))
    return jax.shard_map(local, mesh=mesh, in_specs=in_specs, out_specs=out_specs, check_vma=False)
```

profile of v0, /device:TPU:92, one launch (start us, length us, event | category | flops | bytes accessed | tf_op | source)
XLA Modules:
  0.0 155.5 jit_solution(11269415672865246315)
XLA Ops:
  0.7 1.5 reshape.799
  2.1 2.1 %dynamic-slice_reduce_fusion = (bf16[64,16,128]{2,1,0:T(8,128)(2,1)S(1)}, bf16[1,64,16,1,128]{4,3,2,1,0:T(2,128)(2,1)S(1)}) fusion(bf16[1,64,16,2,128]{4,3,2,1,0:T(2,128)(2,1)S(1)} %reshape.799, s32[]{:T(128)S(6)} %select_n.37, s32[]{:T(128)S(6)} %select_n.38), kind=kLoop, calls=%fused_computation.67 | loop fusion | bytes 1048584 | tf_op jit(solution)/shard_map/jit(dynamic_index_in_dim)/dynamic_slice | solution.py:186
  4.3 2.0 %collective-permute-start = (bf16[1,64,16,128]{3,2,1,0:T(8,128)(2,1)S(1)}, bf16[1,64,16,128]{3,2,1,0:T(8,128)(2,1)}, u32[]{:S(2)}, u32[]{:S(2)}) collective-permute-start(bf16[1,64,16,128]{3,2,1,0:T(8,128)(2,1)S(1)} %bitcast.318), channel_id=1, source_target_pairs={{0,1},{1,0},{2,3},{3,2},{4,5},{5,4},{6,7},{7,6},{8,9},{9,8},{10,11... | collective-permute-start | bytes 786440 | tf_op jit(solution)/shard_map/ppermute | solution.py:65
  6.9 0.1 fusion.88
  7.1 0.1 convert_multiply_fusion
  7.2 0.6 fusion.132
  7.8 0.6 fusion.133
  8.4 70.1 %all-gather = bf16[384,4,128]{2,0,1:T(8,128)(2,1)S(1)} all-gather(bf16[24,4,128]{2,0,1:T(8,128)(2,1)S(1)} %copy.110), channel_id=2, replica_groups=mesh['grp'=2,'dp'=8,'kv'=16,'tp'=2] {'kv'}, dimensions={0}, use_global_device_ids=true | all-gather | bytes 417792 | tf_op jit(solution)/shard_map/all_gather | solution.py:21
  78.5 2.4 %all_gather.16 = bf16[32,24,4,128]{3,1,0,2:T(8,128)(2,1)S(1)} all-gather(bf16[16,24,4,128]{3,1,0,2:T(8,128)(2,1)S(1)} %bitcast.308), channel_id=1, replica_groups=mesh['grp'=2,'dp'=8,'kv'=16,'tp'=2] {'tp'}, dimensions={0}, use_global_device_ids=true | all-gather | bytes 1179648 | tf_op jit(solution)/shard_map/all_gather | solution.py:21
  80.9 0.1 convert_element_type.149
  81.0 0.2 copy.112
  81.2 0.2 multiply_reduce_fusion
  81.4 0.1 copy.114
  81.5 0.7 rsqrt.46
  82.2 0.3 fusion.5
  82.5 0.3 copy.115
  82.8 0.4 convolution_convert_fusion.2
  83.2 0.1 copy.118
  83.3 1.5 convolution_convert_fusion.3
  84.8 0.1 copy.117
  85.0 0.1 copy.119
  85.0 2.1 %all_gather.17 = bf16[128,192]{1,0:T(8,128)(2,1)S(1)} all-gather(bf16[64,192]{1,0:T(8,128)(2,1)S(1)} %copy.119), channel_id=1, replica_groups=mesh['grp'=2,'dp'=8,'kv'=16,'tp'=2] {'tp'}, dimensions={0}, use_global_device_ids=true | all-gather | bytes 73728 | tf_op jit(solution)/shard_map/all_gather | solution.py:35
  87.1 1.5 fusion.3
  88.6 2.1 %fusion.4 = f32[96,64]{0,1:T(8,128)} fusion(bf16[1,64,4096]{2,1,0:T(8,128)(2,1)} %param.21, bf16[12,8,32,128]{3,2,1,0:T(8,128)(2,1)S(1)} %bitcast.313), kind=kOutput, calls=%fused_computation.12 | convolution fusion | flops 50343936 | bytes 1335296 | tf_op jit(solution)/shard_map/dot_general | solution.py:121
  90.7 0.8 copy.116
  91.7 0.1 slice_convert_fusion
  91.9 0.1 multiply_reduce_fusion.1
  92.0 0.1 multiply_multiply_fusion
  92.2 0.1 multiply_reduce_fusion.2
  92.3 0.1 broadcast_multiply_fusion
  92.5 0.9 copy.113
  93.5 1.2 fusion.1
  94.8 0.3 fusion.135
  95.1 0.3 fusion.134
  95.5 0.1 reshape.774
  95.6 0.2 fusion.101
  95.9 0.1 div.54
  96.0 0.2 slice_reduce_fusion
  96.2 1.4 fusion.32
  97.7 1.5 fusion.30
  99.3 1.7 %fusion.28 = f32[24,1,64]{2,1,0:T(1,128)S(1)} fusion(f32[24]{0:T(128)S(1)} %get-tuple-element.38, f32[24,128]{1,0:T(8,128)S(1)} %bitcast.333, f32[24,64]{1,0:T(8,128)S(1)} %subtract_multiply_fusion.6, f32[24,4,1,128]{3,1,2,0:T(4,128)S(1)} %convert_multiply_fusion, f32[24,1,64,128]{3,2,1,0:T(8,128)S(1)} %copy-done.1, f32[24]{0:T(128)S(1)} %get-tuple-element.40, ...), kind=kOutput, calls=%fused_computation.36 | convolution fusion | flops 3735552 | bytes 855552 | tf_op jit(solution)/shard_map/shed,shd->she/dot_general | solution.py:86
  101.1 2.3 %fusion.26 = f32[24,1,64]{2,1,0:T(1,128)S(1)} fusion(f32[24]{0:T(128)S(1)} %get-tuple-element.39, f32[24,128]{1,0:T(8,128)S(1)} %bitcast.330, f32[24,64]{1,0:T(8,128)S(1)} %subtract_multiply_fusion.5, f32[24]{0:T(128)S(1)} %get-tuple-element.38, f32[24,128]{1,0:T(8,128)S(1)} %bitcast.334, f32[24,64]{1,0:T(8,128)S(1)} %subtract_multiply_fusion.6, ...), kind=kOutput, calls=%fused_computation.34 | convolution fusion | flops 4325376 | bytes 880640 | tf_op jit(solution)/shard_map/shed,shd->she/dot_general | solution.py:86
  103.4 1.2 multiply_add_fusion.3
  104.7 1.4 fusion.24
  106.1 1.4 fusion.22
  107.6 1.5 fusion.20
  109.1 1.8 %multiply_add_fusion.1 = f32[24,1,64,128]{3,2,1,0:T(8,128)S(1)} fusion(f32[24,128]{1,0:T(8,128)S(1)} %bitcast.349, f32[24,64]{1,0:T(8,128)S(1)} %subtract_multiply_fusion.2, f32[24]{0:T(128)S(1)} %get-tuple-element.8, f32[24,128]{1,0:T(8,128)S(1)} %bitcast.339, f32[24,64]{1,0:T(8,128)S(1)} %subtract_multiply_fusion.3, f32[24]{0:T(128)S(1)} %get-tuple-element.9, ...), kind=kLoop, calls=%fused_computation.45 | loop fusion | flops 3538944 | bytes 1684032 | tf_op jit(solution)/shard_map/add | solution.py:88
  110.9 1.3 fusion.18
  112.2 1.4 fusion.16
  113.7 1.4 fusion.14
  115.1 1.5 fusion.12
  116.7 1.7 %fusion.10 = f32[24,1,64]{2,1,0:T(1,128)S(1)} fusion(f32[24,1,64,128]{3,2,1,0:T(8,128)S(1)} %multiply_add_fusion.1, f32[24,128]{1,0:T(8,128)S(1)} %bitcast.367, f32[24,64]{1,0:T(8,128)S(1)} %subtract_multiply_fusion, f32[24]{0:T(128)S(1)} %get-tuple-element.7, f32[24,128]{1,0:T(8,128)S(1)} %bitcast.360, f32[24,64]{1,0:T(8,128)S(1)} %subtract_multiply_fusion.1, ...), kind=kOutput, calls=%fused_computation.18 | convolution fusion | flops 3538944 | bytes 855040 | tf_op jit(solution)/shard_map/shed,shd->she/dot_general | solution.py:171
  118.3 0.1 fusion.92
  118.4 1.9 %all-gather.2 = f32[2,24,4]{1,2,0:T(4,128)S(1)} all-gather(f32[1,24,4]{1,2,0:T(4,128)S(1)} %bitcast.373), channel_id=3, replica_groups=mesh['grp'=2,'dp'=8,'kv'=16,'tp'=2] {'tp'}, dimensions={0}, use_global_device_ids=true | all-gather | bytes 1152 | tf_op jit(solution)/shard_map/all_gather | solution.py:44
  120.4 0.1 fusion.91
  120.5 0.7 reshape.862
  121.2 3.3 %all-to-all-start = ((bf16[2,2,3072]{2,1,0:T(2,128)(2,1)}), bf16[2,2,3072]{2,1,0:T(2,128)(2,1)S(1)}, u32[]{:S(2)}, u32[]{:S(2)}) async-start(bf16[2,2,3072]{2,1,0:T(2,128)(2,1)} %reshape.862), calls=%async_computation | async-start | bytes 49152 | tf_op jit(solution)/shard_map/all_to_all | solution.py:50
  124.6 1.3 all-to-all-done
  125.8 0.1 reshape.863
  126.0 0.1 reshape_reshape.3
  126.1 1.0 copy.193
  127.1 0.3 fusion.2
  127.5 27.3 %all_to_all.10 = bf16[16,96,128]{2,1,0:T(8,128)(2,1)S(1)} all-to-all(bf16[16,96,128]{2,1,0:T(8,128)(2,1)S(1)} %bitcast.307), channel_id=1, replica_groups=mesh['grp'=2,'dp'=8,'kv'=16,'tp'=2] {'kv'}, dimensions={0} | all-to-all | bytes 786432 | tf_op jit(solution)/shard_map/all_to_all | solution.py:76
  154.9 0.7 reduce_sum.72
  (79 shorter events, 1.5 us)
Async XLA Ops:
  0.6 82.2 %copy-start = (bf16[1,64,4096]{2,1,0:T(8,128)(2,1)S(1)}, bf16[1,64,4096]{2,1,0:T(8,128)(2,1)}, u32[]{:S(2)}) copy-start(bf16[1,64,4096]{2,1,0:T(8,128)(2,1)} %param.20) | copy-start | bytes 1572868
  2.1 4.8 %copy-start.10 = (bf16[24,4,1,128]{3,1,2,0:T(4,128)(2,1)S(1)}, bf16[24,4,1,128]{3,1,2,0:T(4,128)(2,1)}, u32[]{:S(2)}) copy-start(bf16[24,4,1,128]{3,1,2,0:T(4,128)(2,1)} %param.29) | copy-start | bytes 73732
  2.1 4.9 %copy-start.17 = (bf16[24,4,128]{2,1,0:T(4,128)(2,1)S(1)}, bf16[24,4,128]{2,1,0:T(4,128)(2,1)}, u32[]{:S(2)}) copy-start(bf16[24,4,128]{2,1,0:T(4,128)(2,1)} %param.17) | copy-start | bytes 73732
  2.1 5.7 %copy-start.9 = (bf16[24,4,1,64]{3,1,2,0:T(4,128)(2,1)S(1)}, bf16[24,4,1,64]{3,1,2,0:T(4,128)(2,1)}, u32[]{:S(2)}) copy-start(bf16[24,4,1,64]{3,1,2,0:T(4,128)(2,1)} %param.30) | copy-start | bytes 36868
  4.3 121.8 %collective-permute-start = (bf16[1,64,16,128]{3,2,1,0:T(8,128)(2,1)S(1)}, bf16[1,64,16,128]{3,2,1,0:T(8,128)(2,1)}, u32[]{:S(2)}, u32[]{:S(2)}) collective-permute-start(bf16[1,64,16,128]{3,2,1,0:T(8,128)(2,1)S(1)} %bitcast.318), channel_id=1, source_target_pairs={{0,1},{1,0},{2,3},{3,2},{4,5},{5,4},{6,7},{7,6},{8,9},{9,8},{10,11... | collective-permute-start | bytes 786440 | tf_op jit(solution)/shard_map/ppermute | solution.py:65
  81.2 1.0 copy-start.11
  92.5 1.0 copy-start.12
  92.5 1.0 copy-start.20
  93.4 1.3 copy-start.3
  93.5 1.7 %copy-start.4 = (bf16[4096,16]{0,1:T(8,128)(2,1)S(1)}, bf16[4096,16]{0,1:T(8,128)(2,1)}, u32[]{:S(2)}) copy-start(bf16[4096,16]{0,1:T(8,128)(2,1)} %param.23) | copy-start | bytes 393220
  94.7 1.4 copy-start.18
  94.7 1.4 copy-start.19
  94.8 1.4 copy-start.22
  94.8 1.5 copy-start.1
  94.8 2.9 %copy-start.16 = (f32[24,1,1,64]{3,1,2,0:T(1,128)S(1)}, f32[24,1,1,64]{3,1,2,0:T(1,128)}, u32[]{:S(2)}) copy-start(f32[24,1,1,64]{3,1,2,0:T(1,128)} %get-tuple-element.26) | copy-start | bytes 18436
  94.8 2.9 %copy-start.5 = (f32[24,1,1,128]{3,1,2,0:T(1,128)S(1)}, f32[24,1,1,128]{3,1,2,0:T(1,128)}, u32[]{:S(2)}) copy-start(f32[24,1,1,128]{3,1,2,0:T(1,128)} %get-tuple-element.22) | copy-start | bytes 36868
  95.1 4.1 %copy-start.15 = (f32[24,1,1,64]{3,1,2,0:T(1,128)S(1)}, f32[24,1,1,64]{3,1,2,0:T(1,128)}, u32[]{:S(2)}) copy-start(f32[24,1,1,64]{3,1,2,0:T(1,128)} %get-tuple-element.27) | copy-start | bytes 18436
  95.1 4.2 %copy-start.8 = (f32[24,1,1,128]{3,1,2,0:T(1,128)S(1)}, f32[24,1,1,128]{3,1,2,0:T(1,128)}, u32[]{:S(2)}) copy-start(f32[24,1,1,128]{3,1,2,0:T(1,128)} %get-tuple-element.25) | copy-start | bytes 36868
  97.6 3.3 %copy-start.14 = (f32[24,1,1,64]{3,1,2,0:T(1,128)S(1)}, f32[24,1,1,64]{3,1,2,0:T(1,128)}, u32[]{:S(2)}) copy-start(f32[24,1,1,64]{3,1,2,0:T(1,128)} %get-tuple-element.28) | copy-start | bytes 18436
  97.6 3.4 %copy-start.7 = (f32[24,1,1,128]{3,1,2,0:T(1,128)S(1)}, f32[24,1,1,128]{3,1,2,0:T(1,128)}, u32[]{:S(2)}) copy-start(f32[24,1,1,128]{3,1,2,0:T(1,128)} %get-tuple-element.24) | copy-start | bytes 36868
  101.0 2.4 %copy-start.13 = (f32[24,1,1,64]{3,1,2,0:T(1,128)S(1)}, f32[24,1,1,64]{3,1,2,0:T(1,128)}, u32[]{:S(2)}) copy-start(f32[24,1,1,64]{3,1,2,0:T(1,128)} %get-tuple-element.29) | copy-start | bytes 18436
  101.0 2.5 %copy-start.6 = (f32[24,1,1,128]{3,1,2,0:T(1,128)S(1)}, f32[24,1,1,128]{3,1,2,0:T(1,128)}, u32[]{:S(2)}) copy-start(f32[24,1,1,128]{3,1,2,0:T(1,128)} %get-tuple-element.23) | copy-start | bytes 36868
  104.6 6.2 %copy-start.2 = (f32[24,1,64,128]{3,2,1,0:T(8,128)}, f32[24,1,64,128]{3,2,1,0:T(8,128)S(1)}, u32[]{:S(2)}) copy-start(f32[24,1,64,128]{3,2,1,0:T(8,128)S(1)} %multiply_add_fusion.3) | copy-start | bytes 2359300
  115.1 5.2 %copy-start.21 = (f32[64]{0:T(128)S(1)}, f32[64]{0:T(128)}, u32[]{:S(2)}) copy-start(f32[64]{0:T(128)} %param.26) | copy-start | bytes 772
  121.2 4.6 %all-to-all-start = ((bf16[2,2,3072]{2,1,0:T(2,128)(2,1)}), bf16[2,2,3072]{2,1,0:T(2,128)(2,1)S(1)}, u32[]{:S(2)}, u32[]{:S(2)}) async-start(bf16[2,2,3072]{2,1,0:T(2,128)(2,1)} %reshape.862), calls=%async_computation | async-start | bytes 49152 | tf_op jit(solution)/shard_map/all_to_all | solution.py:50
where the time goes:
time: 156 us
  blocking collectives  104 us (67%)
  matrix products  24.8 us (16%)
  local copies, waits for them, and re-layouts  11.2 us (7%)
  other arithmetic  7.28 us (5%)
  starting transfers between devices  5.23 us (3%)
  between operations  1.92 us (1%)
    all_gather x2, blocking collectives, gather_in_order(): parts = lax.all_gather(parts, axes[k], axis=0, tiled=True)  72.5 us
    all_to_all x1, blocking collectives, sum_at_owner(): lax.all_to_all(parts, axis, split_axis=0, concat_axis=0, tiled=True)  27.3 us
    dot_general x8, matrix products, delta_update(): jnp.einsum('shed,shd->she', carried, keys_now, precision=PRECISE)  12.6 us
    dot_general x4, matrix products, local(): jnp.einsum('shed,shd->she', carried, queries[:, position], precision=PREC...  5.88 us
    dot_general x4, matrix products, project(): lax.dot_general(flat_rows, weight.reshape(-1, width), (((1,), (1,)), ((),...  5.44 us
    all_to_all x1, starting transfers between devices, from_everyone(): return lax.all_to_all(copies, axis, split_axis=0, concat_axis=0, tiled=True)  3.28 us
  transfers between devices with their start and end apart: 2, of which 1 were waited for; matrix products, arithmetic and copies ran while one was open for 24% of the time, Pallas kernels for 0%

commit v1 on v0

--- a/solution.py
+++ b/solution.py
@@ -18,7 +18,9 @@
 def gather_in_order(array, axes, sequence):
     parts = array[None]
     for k in sequence:
-        parts = lax.all_gather(parts, axes[k], axis=0, tiled=True)
+        parts = jnp.concatenate(
+            lax.all_to_all(jnp.stack([parts] * lax.axis_size(axes[k])), axes[k], 0, 0), axis=0
+        )
     current = [lax.axis_size(axes[k]) for k in reversed(sequence)]
     parts = parts.reshape(*current, *array.shape)
     turned = sorted(range(len(sequence)), key=lambda place: sequence[len(sequence) - 1 - place])

time: 156 us -> 142 us (0.910)
  the two profiles are of different devices: /device:TPU:92 before, /device:TPU:94 now
where the time goes in v1:
time: 142 us; the launch traced here: 141 us
  starting transfers between devices  45.6 us (32%)
  blocking collectives  42.1 us (30%)
  matrix products  24.8 us (17%)
  local copies, waits for them, and re-layouts  10.2 us (7%)
  other arithmetic  8.68 us (6%)
  waiting for transfers between devices  8.04 us (6%)
  between operations  1.97 us (1%)
    all_to_all x1, starting transfers between devices, gather_in_order(): lax.all_to_all(jnp.stack([parts] * lax.axis_size(axes[k])), axes[k], 0, 0)  43.7 us
    all_to_all x1, blocking collectives, sum_at_owner(): lax.all_to_all(parts, axis, split_axis=0, concat_axis=0, tiled=True)  30 us
    dot_general x8, matrix products, delta_update(): jnp.einsum('shed,shd->she', carried, keys_now, precision=PRECISE)  12.4 us
    all_to_all x1, waiting for transfers between devices, gather_in_order(): lax.all_to_all(jnp.stack([parts] * lax.axis_size(axes[k])), axes[k], 0, 0)  8.04 us
    dot_general x4, matrix products, local(): jnp.einsum('shed,shd->she', carried, queries[:, position], precision=PREC...  5.89 us
    dot_general x4, matrix products, project(): lax.dot_general(flat_rows, weight.reshape(-1, width), (((1,), (1,)), ((),...  5.55 us
    all_to_all x1, blocking collectives, gather_in_order(): lax.all_to_all(jnp.stack([parts] * lax.axis_size(axes[k])), axes[k], 0, 0)  4.38 us
    add x2, other arithmetic, delta_update(): return carried + update[..., :, None] * keys_now[..., None, :]  4.19 us
  transfers between devices with their start and end apart: 2, of which 1 were waited for; matrix products, arithmetic and copies ran while one was open for 9% of the time, Pallas kernels for 0%

profile of v1, /device:TPU:94, one launch (start us, length us, event | category | flops | bytes accessed | tf_op | source)
XLA Modules:
  0.0 141.5 jit_solution(12007246569175899592)
XLA Ops:
  0.7 0.8 copy.95
  1.5 0.8 stack.31
  2.3 43.7 %all-to-all-start = ((bf16[16,1,24,4,128]{4,2,3,1,0:T(8,128)(2,1)}), bf16[16,1,24,4,128]{4,2,3,1,0:T(8,128)(2,1)S(1)}, u32[]{:S(2)}, u32[]{:S(2)}) async-start(bf16[16,1,24,4,128]{4,2,3,1,0:T(8,128)(2,1)} %stack.31), calls=%async_computation | async-start | bytes 786432 | tf_op jit(solution)/shard_map/all_to_all | solution.py:22
  46.0 0.4 reshape.797
  46.4 2.1 %dynamic-slice_reduce_fusion = (bf16[64,16,128]{2,1,0:T(8,128)(2,1)S(1)}, bf16[1,64,16,1,128]{4,3,2,1,0:T(2,128)(2,1)S(1)}) fusion(bf16[1,64,16,2,128]{4,3,2,1,0:T(2,128)(2,1)S(1)} %reshape.797, s32[]{:T(128)S(6)} %select_n.37, s32[]{:T(128)S(6)} %select_n.38), kind=kLoop, calls=%fused_computation.69 | loop fusion | bytes 1048584 | tf_op jit(solution)/shard_map/jit(dynamic_index_in_dim)/dynamic_slice | solution.py:188
  48.6 2.0 %collective-permute-start = (bf16[1,64,16,128]{3,2,1,0:T(8,128)(2,1)S(1)}, bf16[1,64,16,128]{3,2,1,0:T(8,128)(2,1)S(1)}, u32[]{:S(2)}, u32[]{:S(2)}) collective-permute-start(bf16[1,64,16,128]{3,2,1,0:T(8,128)(2,1)S(1)} %bitcast.316), channel_id=1, source_target_pairs={{0,1},{1,0},{2,3},{3,2},{4,5},{5,4},{6,7},{7,6},{8,9},{9,8},{10,11... | collective-permute-start | bytes 786440 | tf_op jit(solution)/shard_map/ppermute | solution.py:67
  50.5 0.1 fusion.88
  50.7 0.1 convert_multiply_fusion
  50.9 1.4 fusion.32
  52.4 1.5 %fusion.30 = f32[24,1,64]{2,1,0:T(1,128)S(1)} fusion(f32[24,4,1,128]{3,1,2,0:T(4,128)S(1)} %convert_multiply_fusion, f32[24,1,64,128]{3,2,1,0:T(8,128)S(1)} %copy-done.1, f32[24]{0:T(128)S(1)} %get-tuple-element.40, f32[24,128]{1,0:T(8,128)S(1)} %bitcast.322, f32[24,64]{1,0:T(8,128)S(1)} %subtract_multiply_fusion.7, f32[24]{0:T(128)S(1)} %get-tuple-element.41), kind=kOutput, calls=%fused_computation.39 | convolution fusion | flops 3145728 | bytes 830464 | tf_op jit(solution)/shard_map/shed,shd->she/dot_general | solution.py:88
  54.7 1.7 %fusion.28 = f32[24,1,64]{2,1,0:T(1,128)S(1)} fusion(f32[24]{0:T(128)S(1)} %get-tuple-element.38, f32[24,128]{1,0:T(8,128)S(1)} %bitcast.332, f32[24,64]{1,0:T(8,128)S(1)} %subtract_multiply_fusion.6, f32[24,4,1,128]{3,1,2,0:T(4,128)S(1)} %convert_multiply_fusion, f32[24,1,64,128]{3,2,1,0:T(8,128)S(1)} %copy-done.1, f32[24]{0:T(128)S(1)} %get-tuple-element.40, ...), kind=kOutput, calls=%fused_computation.37 | convolution fusion | flops 3735552 | bytes 855552 | tf_op jit(solution)/shard_map/shed,shd->she/dot_general | solution.py:88
  56.5 2.1 %fusion.26 = f32[24,1,64]{2,1,0:T(1,128)S(1)} fusion(f32[24]{0:T(128)S(1)} %get-tuple-element.39, f32[24,128]{1,0:T(8,128)S(1)} %bitcast.329, f32[24,64]{1,0:T(8,128)S(1)} %subtract_multiply_fusion.5, f32[24]{0:T(128)S(1)} %get-tuple-element.38, f32[24,128]{1,0:T(8,128)S(1)} %bitcast.333, f32[24,64]{1,0:T(8,128)S(1)} %subtract_multiply_fusion.6, ...), kind=kOutput, calls=%fused_computation.35 | convolution fusion | flops 4325376 | bytes 880640 | tf_op jit(solution)/shard_map/shed,shd->she/dot_general | solution.py:88
  58.7 2.2 %multiply_add_fusion.3 = f32[24,1,64,128]{3,2,1,0:T(8,128)} fusion(f32[24,128]{1,0:T(8,128)S(1)} %bitcast.327, f32[24,64]{1,0:T(8,128)S(1)} %subtract_multiply_fusion.4, f32[24]{0:T(128)S(1)} %get-tuple-element.39, f32[24,128]{1,0:T(8,128)S(1)} %bitcast.330, f32[24,64]{1,0:T(8,128)S(1)} %subtract_multiply_fusion.5, f32[24]{0:T(128)S(1)} %get-tuple-element.38, ...), kind=kLoop, calls=%fused_computation.49 | loop fusion | flops 2359296 | bytes 1646976 | tf_op jit(solution)/shard_map/add | solution.py:90
  60.9 0.8 copy.177
  61.6 8.0 %all-to-all-done = bf16[16,1,24,4,128]{4,2,3,1,0:T(8,128)(2,1)S(1)} async-done(((bf16[16,1,24,4,128]{4,2,3,1,0:T(8,128)(2,1)}), bf16[16,1,24,4,128]{4,2,3,1,0:T(8,128)(2,1)S(1)}, u32[]{:S(2)}, u32[]{:S(2)}) %all-to-all-start) | async-done | bytes 393248 | tf_op jit(solution)/shard_map/all_to_all | solution.py:22
  69.8 4.4 %all_to_all.20 = bf16[2,16,24,4,128]{4,2,3,1,0:T(8,128)(2,1)S(1)} all-to-all(bf16[2,16,24,4,128]{4,2,3,1,0:T(8,128)(2,1)S(1)} %pad_maximum_fusion), channel_id=1, replica_groups=mesh['grp'=2,'dp'=8,'kv'=16,'tp'=2] {'tp'}, dimensions={0} | all-to-all | bytes 1572864 | tf_op jit(solution)/shard_map/all_to_all | solution.py:22
  74.1 0.2 copy_convert_fusion
  74.3 0.2 multiply_reduce_fusion
  74.5 0.1 copy.98
  74.6 0.7 rsqrt.46
  75.3 0.3 fusion.5
  75.6 0.3 copy.99
  75.9 0.9 copy-done.3
  76.8 0.4 convolution_convert_fusion.2
  77.2 0.1 copy.102
  77.3 1.7 %convolution_convert_fusion.3 = bf16[96,64]{0,1:T(8,128)(2,1)S(1)} fusion(bf16[1,64,4096]{2,1,0:T(8,128)(2,1)} %param.19, bf16[12,8,32,128]{3,2,1,0:T(8,128)(2,1)} %bitcast.309), kind=kOutput, calls=%fused_computation.10 | convolution fusion | flops 50337792 | bytes 1323008 | tf_op jit(solution)/shard_map/dot_general | solution.py:123
  79.1 0.1 copy.101
  79.2 0.1 copy.103
  79.3 2.1 %all_gather.9 = bf16[128,192]{1,0:T(8,128)(2,1)S(1)} all-gather(bf16[64,192]{1,0:T(8,128)(2,1)S(1)} %copy.103), channel_id=1, replica_groups=mesh['grp'=2,'dp'=8,'kv'=16,'tp'=2] {'tp'}, dimensions={0}, use_global_device_ids=true | all-gather | bytes 73728 | tf_op jit(solution)/shard_map/all_gather | solution.py:37
  81.4 1.7 %fusion.3 = f32[96,64]{0,1:T(8,128)S(1)} fusion(bf16[1,64,4096]{2,1,0:T(8,128)(2,1)} %param.22, bf16[12,8,32,128]{3,2,1,0:T(8,128)(2,1)} %bitcast.310), kind=kOutput, calls=%fused_computation.8 | convolution fusion | flops 50343936 | bytes 1335296 | tf_op jit(solution)/shard_map/dot_general | solution.py:123
  83.1 1.7 %fusion.4 = f32[96,64]{0,1:T(8,128)S(1)} fusion(bf16[1,64,4096]{2,1,0:T(8,128)(2,1)} %param.21, bf16[12,8,32,128]{3,2,1,0:T(8,128)(2,1)} %bitcast.311), kind=kOutput, calls=%fused_computation.12 | convolution fusion | flops 50343936 | bytes 1335296 | tf_op jit(solution)/shard_map/dot_general | solution.py:123
  84.9 0.6 fusion.130
  85.6 0.1 slice_convert_fusion
  85.8 0.1 multiply_reduce_fusion.1
  86.0 0.1 multiply_multiply_fusion
  86.1 0.1 multiply_reduce_fusion.2
  86.3 0.1 broadcast_multiply_fusion
  86.5 0.9 copy.97
  87.4 1.2 fusion.1
  88.7 0.3 fusion.135
  89.0 0.3 fusion.134
  89.4 0.1 reshape.772
  89.5 0.2 fusion.101
  89.8 0.1 div.54
  89.9 0.2 slice_reduce_fusion
  90.1 1.4 fusion.24
  91.6 1.5 %fusion.22 = f32[24,1,64]{2,1,0:T(1,128)S(1)} fusion(f32[24,1,64,128]{3,2,1,0:T(8,128)S(1)} %copy-done.2, f32[24,128]{1,0:T(8,128)S(1)} %bitcast.336, f32[24,64]{1,0:T(8,128)S(1)} %subtract_multiply_fusion.3, f32[24]{0:T(128)S(1)} %get-tuple-element.9, f32[24,4,1,128]{3,1,0,2:T(4,128)S(1)} %multiply_multiply_fusion), kind=kOutput, calls=%fused_computation.31 | convolution fusion | flops 2949120 | bytes 829952 | tf_op jit(solution)/shard_map/shed,shd->she/dot_general | solution.py:173
  93.0 1.5 %fusion.20 = f32[24,1,64]{2,1,0:T(1,128)S(1)} fusion(f32[24,1,64,128]{3,2,1,0:T(8,128)S(1)} %copy-done.2, f32[24]{0:T(128)S(1)} %get-tuple-element.8, f32[24,128]{1,0:T(8,128)S(1)} %bitcast.337, f32[24,64]{1,0:T(8,128)S(1)} %subtract_multiply_fusion.3, f32[24]{0:T(128)S(1)} %get-tuple-element.9, f32[24,4,1,128]{3,1,0,2:T(4,128)S(1)} %broadcast_multiply_fusion), kind=kOutput, calls=%fused_computation.29 | convolution fusion | flops 3145728 | bytes 830464 | tf_op jit(solution)/shard_map/shed,shd->she/dot_general | solution.py:88
  94.6 2.0 %multiply_add_fusion.1 = f32[24,1,64,128]{3,2,1,0:T(8,128)S(1)} fusion(f32[24,128]{1,0:T(8,128)S(1)} %bitcast.348, f32[24,64]{1,0:T(8,128)S(1)} %subtract_multiply_fusion.2, f32[24]{0:T(128)S(1)} %get-tuple-element.8, f32[24,128]{1,0:T(8,128)S(1)} %bitcast.338, f32[24,64]{1,0:T(8,128)S(1)} %subtract_multiply_fusion.3, f32[24]{0:T(128)S(1)} %get-tuple-element.9, ...), kind=kLoop, calls=%fused_computation.47 | loop fusion | flops 3538944 | bytes 1684032 | tf_op jit(solution)/shard_map/add | solution.py:90
  96.6 1.3 fusion.18
  98.0 1.4 fusion.16
  99.4 1.4 %fusion.14 = f32[24,1,64]{2,1,0:T(1,128)S(1)} fusion(f32[24,1,64,128]{3,2,1,0:T(8,128)S(1)} %multiply_add_fusion.1, f32[24,128]{1,0:T(8,128)S(1)} %bitcast.357, f32[24,64]{1,0:T(8,128)S(1)} %subtract_multiply_fusion.1, f32[24]{0:T(128)S(1)} %get-tuple-element.6, f32[24,4,1,128]{3,1,0,2:T(4,128)S(1)} %multiply_multiply_fusion), kind=kOutput, calls=%fused_computation.23 | convolution fusion | flops 2949120 | bytes 829952 | tf_op jit(solution)/shard_map/shed,shd->she/dot_general | solution.py:173
  100.9 1.5 %fusion.12 = f32[24,1,64]{2,1,0:T(1,128)S(1)} fusion(f32[24,1,64,128]{3,2,1,0:T(8,128)S(1)} %multiply_add_fusion.1, f32[24]{0:T(128)S(1)} %get-tuple-element.7, f32[24,128]{1,0:T(8,128)S(1)} %bitcast.358, f32[24,64]{1,0:T(8,128)S(1)} %subtract_multiply_fusion.1, f32[24]{0:T(128)S(1)} %get-tuple-element.6, f32[24,4,1,128]{3,1,0,2:T(4,128)S(1)} %broadcast_multiply_fusion), kind=kOutput, calls=%fused_computation.21 | convolution fusion | flops 3145728 | bytes 830464 | tf_op jit(solution)/shard_map/shed,shd->she/dot_general | solution.py:88
  102.4 1.7 %fusion.10 = f32[24,1,64]{2,1,0:T(1,128)S(1)} fusion(f32[24,1,64,128]{3,2,1,0:T(8,128)S(1)} %multiply_add_fusion.1, f32[24,128]{1,0:T(8,128)S(1)} %bitcast.366, f32[24,64]{1,0:T(8,128)S(1)} %subtract_multiply_fusion, f32[24]{0:T(128)S(1)} %get-tuple-element.7, f32[24,128]{1,0:T(8,128)S(1)} %bitcast.359, f32[24,64]{1,0:T(8,128)S(1)} %subtract_multiply_fusion.1, ...), kind=kOutput, calls=%fused_computation.19 | convolution fusion | flops 3538944 | bytes 855040 | tf_op jit(solution)/shard_map/shed,shd->she/dot_general | solution.py:173
  104.1 0.1 fusion.92
  104.2 1.9 %all-gather.1 = f32[2,24,4]{1,2,0:T(4,128)S(1)} all-gather(f32[1,24,4]{1,2,0:T(4,128)S(1)} %bitcast.372), channel_id=2, replica_groups=mesh['grp'=2,'dp'=8,'kv'=16,'tp'=2] {'tp'}, dimensions={0}, use_global_device_ids=true | all-gather | bytes 1152 | tf_op jit(solution)/shard_map/all_gather | solution.py:46
  106.1 0.1 fusion.91
  106.2 0.1 reshape.857
  106.3 3.8 %all_to_all.21 = bf16[2,2,3072]{2,1,0:T(2,128)(2,1)S(1)} all-to-all(bf16[2,2,3072]{2,1,0:T(2,128)(2,1)S(1)} %reshape.857), channel_id=1, replica_groups=mesh['grp'=2,'dp'=8,'kv'=16,'tp'=2] {'tp'}, dimensions={0} | all-to-all | bytes 49152 | tf_op jit(solution)/shard_map/all_to_all | solution.py:52
  110.1 0.1 reshape.858
  110.3 0.1 reshape_reshape.3
  110.4 0.3 fusion.2
  110.7 30.0 %all_to_all.22 = bf16[16,96,128]{2,1,0:T(8,128)(2,1)S(1)} all-to-all(bf16[16,96,128]{2,1,0:T(8,128)(2,1)S(1)} %bitcast.305), channel_id=1, replica_groups=mesh['grp'=2,'dp'=8,'kv'=16,'tp'=2] {'kv'}, dimensions={0} | all-to-all | bytes 786432 | tf_op jit(solution)/shard_map/all_to_all | solution.py:78
  140.8 0.7 reduce_sum.72
  (92 shorter events, 1.7 us)
Async XLA Ops:
  0.6 76.2 %copy-start = (bf16[1,64,4096]{2,1,0:T(8,128)(2,1)S(1)}, bf16[1,64,4096]{2,1,0:T(8,128)(2,1)}, u32[]{:S(2)}) copy-start(bf16[1,64,4096]{2,1,0:T(8,128)(2,1)} %param.20) | copy-start | bytes 1572868
  0.6 45.3 %copy-start.4 = (bf16[1,64,4096]{2,1,0:T(8,128)(2,1)S(1)}, bf16[1,64,4096]{2,1,0:T(8,128)(2,1)}, u32[]{:S(2)}) copy-start(bf16[1,64,4096]{2,1,0:T(8,128)(2,1)} %param.27) | copy-start | bytes 1572868
  2.3 67.4 %all-to-all-start = ((bf16[16,1,24,4,128]{4,2,3,1,0:T(8,128)(2,1)}), bf16[16,1,24,4,128]{4,2,3,1,0:T(8,128)(2,1)S(1)}, u32[]{:S(2)}, u32[]{:S(2)}) async-start(bf16[16,1,24,4,128]{4,2,3,1,0:T(8,128)(2,1)} %stack.31), calls=%async_computation | async-start | bytes 786432 | tf_op jit(solution)/shard_map/all_to_all | solution.py:22
  46.3 4.2 %copy-start.13 = (bf16[24,4,1,128]{3,1,2,0:T(4,128)(2,1)S(1)}, bf16[24,4,1,128]{3,1,2,0:T(4,128)(2,1)}, u32[]{:S(2)}) copy-start(bf16[24,4,1,128]{3,1,2,0:T(4,128)(2,1)} %param.29) | copy-start | bytes 73732
  46.4 4.4 %copy-start.12 = (bf16[24,4,1,64]{3,1,2,0:T(4,128)(2,1)S(1)}, bf16[24,4,1,64]{3,1,2,0:T(4,128)(2,1)}, u32[]{:S(2)}) copy-start(bf16[24,4,1,64]{3,1,2,0:T(4,128)(2,1)} %param.30) | copy-start | bytes 36868
  46.4 4.5 %copy-start.24 = (f32[24,4,1]{0,2,1:T(1,128)S(1)}, f32[24,4,1]{0,2,1:T(1,128)}, u32[]{:S(2)}) copy-start(f32[24,4,1]{0,2,1:T(1,128)} %param.32) | copy-start | bytes 1156
  46.4 4.5 %copy-start.25 = (f32[24,4,1]{0,2,1:T(1,128)S(1)}, f32[24,4,1]{0,2,1:T(1,128)}, u32[]{:S(2)}) copy-start(f32[24,4,1]{0,2,1:T(1,128)} %param.31) | copy-start | bytes 1156
  46.4 4.5 %copy-start.28 = (s32[24]{0:T(128)S(1)}, s32[24]{0:T(128)}, u32[]{:S(2)}) copy-start(s32[24]{0:T(128)} %param.33) | copy-start | bytes 292
  46.4 4.5 %copy-start.1 = (f32[24,1,64,128]{3,2,1,0:T(8,128)S(1)}, f32[24,1,64,128]{3,2,1,0:T(8,128)}, u32[]{:S(2)}) copy-start(f32[24,1,64,128]{3,2,1,0:T(8,128)} %param.28) | copy-start | bytes 2359300
  48.6 12.3 %collective-permute-start = (bf16[1,64,16,128]{3,2,1,0:T(8,128)(2,1)S(1)}, bf16[1,64,16,128]{3,2,1,0:T(8,128)(2,1)S(1)}, u32[]{:S(2)}, u32[]{:S(2)}) collective-permute-start(bf16[1,64,16,128]{3,2,1,0:T(8,128)(2,1)S(1)} %bitcast.316), channel_id=1, source_target_pairs={{0,1},{1,0},{2,3},{3,2},{4,5},{5,4},{6,7},{7,6},{8,9},{9,8},{10,11... | collective-permute-start | bytes 786440 | tf_op jit(solution)/shard_map/ppermute | solution.py:67
  50.9 7.7 %copy-start.20 = (f32[24]{0:T(128)}, f32[24]{0:T(128)S(1)}, u32[]{:S(2)}) copy-start(f32[24]{0:T(128)S(1)} %get-tuple-element.39) | copy-start | bytes 292
  50.9 7.7 %copy-start.22 = (f32[24]{0:T(128)}, f32[24]{0:T(128)S(1)}, u32[]{:S(2)}) copy-start(f32[24]{0:T(128)S(1)} %get-tuple-element.40) | copy-start | bytes 292
  56.4 4.4 %copy-start.8 = (f32[24,64]{1,0:T(8,128)}, f32[24,64]{1,0:T(8,128)S(1)}, u32[]{:S(2)}) copy-start(f32[24,64]{1,0:T(8,128)S(1)} %subtract_multiply_fusion.5) | copy-start | bytes 18436
  58.6 11.1 %copy-start.10 = (f32[24,64]{1,0:T(8,128)}, f32[24,64]{1,0:T(8,128)S(1)}, u32[]{:S(2)}) copy-start(f32[24,64]{1,0:T(8,128)S(1)} %subtract_multiply_fusion.4) | copy-start | bytes 18436
  74.1 1.2 copy-start.14
  75.9 0.9 copy-start.3
  86.4 1.0 copy-start.15
  86.4 1.0 copy-start.26
  87.4 1.3 copy-start.6
  87.4 1.6 %copy-start.7 = (bf16[4096,16]{0,1:T(8,128)(2,1)S(1)}, bf16[4096,16]{0,1:T(8,128)(2,1)}, u32[]{:S(2)}) copy-start(bf16[4096,16]{0,1:T(8,128)(2,1)} %param.23) | copy-start | bytes 393220
  88.7 1.4 %copy-start.2 = (f32[24,1,64,128]{3,2,1,0:T(8,128)S(1)}, f32[24,1,64,128]{3,2,1,0:T(8,128)}, u32[]{:S(2)}) copy-start(f32[24,1,64,128]{3,2,1,0:T(8,128)} %multiply_add_fusion.3) | copy-start | bytes 2359300
  88.7 2.8 %copy-start.19 = (f32[24,1,1,64]{3,1,0,2:T(1,128)S(1)}, f32[24,1,1,64]{3,1,0,2:T(1,128)}, u32[]{:S(2)}) copy-start(f32[24,1,1,64]{3,1,0,2:T(1,128)} %get-tuple-element.17) | copy-start | bytes 18436
  89.3 5.2 %copy-start.18 = (f32[24,1,1,64]{3,1,0,2:T(1,128)S(1)}, f32[24,1,1,64]{3,1,0,2:T(1,128)}, u32[]{:S(2)}) copy-start(f32[24,1,1,64]{3,1,0,2:T(1,128)} %get-tuple-element.16) | copy-start | bytes 18436
  89.3 5.2 %copy-start.9 = (f32[24,64]{1,0:T(8,128)S(1)}, f32[24,64]{1,0:T(8,128)}, u32[]{:S(2)}) copy-start(f32[24,64]{1,0:T(8,128)} %copy-done.8) | copy-start | bytes 18436
  89.3 5.2 %copy-start.11 = (f32[24,64]{1,0:T(8,128)S(1)}, f32[24,64]{1,0:T(8,128)}, u32[]{:S(2)}) copy-start(f32[24,64]{1,0:T(8,128)} %copy-done.10) | copy-start | bytes 18436
  89.4 5.2 %copy-start.21 = (f32[24]{0:T(128)S(1)}, f32[24]{0:T(128)}, u32[]{:S(2)}) copy-start(f32[24]{0:T(128)} %copy-done.20) | copy-start | bytes 292
  89.4 5.2 %copy-start.23 = (f32[24]{0:T(128)S(1)}, f32[24]{0:T(128)}, u32[]{:S(2)}) copy-start(f32[24]{0:T(128)} %copy-done.22) | copy-start | bytes 292
  94.6 4.7 %copy-start.17 = (f32[24,1,1,64]{3,1,0,2:T(1,128)S(1)}, f32[24,1,1,64]{3,1,0,2:T(1,128)}, u32[]{:S(2)}) copy-start(f32[24,1,1,64]{3,1,0,2:T(1,128)} %get-tuple-element.14) | copy-start | bytes 18436
  98.0 4.4 %copy-start.16 = (f32[24,1,1,64]{3,1,0,2:T(1,128)S(1)}, f32[24,1,1,64]{3,1,0,2:T(1,128)}, u32[]{:S(2)}) copy-start(f32[24,1,1,64]{3,1,0,2:T(1,128)} %get-tuple-element.15) | copy-start | bytes 18436
  100.9 5.2 %copy-start.27 = (f32[64]{0:T(128)S(1)}, f32[64]{0:T(128)}, u32[]{:S(2)}) copy-start(f32[64]{0:T(128)} %param.26) | copy-start | bytes 772
  100.9 9.5 %copy-start.5 = (bf16[8,8,16,128]{3,1,2,0:T(8,128)(2,1)S(1)}, bf16[8,8,16,128]{3,1,2,0:T(8,128)(2,1)}, u32[]{:S(2)}) copy-start(bf16[8,8,16,128]{3,1,2,0:T(8,128)(2,1)} %copy.177) | copy-start | bytes 786436
